TPU v7x, 32 devices: a whole 2x2x4 slice. The times are simulated.
32 devices in a mesh: sp: 8 (over z, core), tp: 4 (over y, x).
Axes of the slice: x: 2, y: 2, z: 4, core: 2. Of those that a mesh axis runs over, the one named last changes fastest.
Arguments:
- u_val: bfloat16 [2048, 2048], P('sp', 'tp'), may hold values from -6 to 6
- u_gate: bfloat16 [2048, 2048], P('sp', 'tp'), may hold values from -9 to 9
- conv_weight: float32 [31, 2048], P(None, 'tp')
- conv_bias: float32 [2048], P('tp'), may hold values from -3 to 3
- ln_gain: float32 [2048], P('tp'), may hold values from 0.1 to 1.9
- ln_bias: float32 [2048], P('tp'), may hold values from -3 to 3
- proj_weight: bfloat16 [2048, 4096], P(None, 'tp'), may hold values from -0.125 to 0.125
- resid: bfloat16 [2048, 4096], P('sp', 'tp')
- norm_gain: float32 [4096], P('tp'), may hold values from 0.1 to 1.9
- route_ids: int32 [2048, 2], P('sp'), may hold values from 0 to 7, all different within a row; in each aligned block of 256 rows (0 to 255, 256 to 511, ...) at most 128 rows name the same one
- route_wts: float32 [2048, 2], P('sp'), may hold values from 0.3 to 1.5
- expert_gate: bfloat16 [8, 4096, 1024], P('sp', None, 'tp'), may hold values from -0.09375 to 0.09375
- expert_up: bfloat16 [8, 4096, 1024], P('sp', None, 'tp'), may hold values from -0.09375 to 0.09375
- expert_down: bfloat16 [8, 1024, 4096], P('sp', None, 'tp'), may hold values from -0.1875 to 0.1875
- shared_gate: bfloat16 [4096, 1024], P(None, 'tp'), may hold values from -0.09375 to 0.09375
- shared_up: bfloat16 [4096, 1024], P(None, 'tp'), may hold values from -0.09375 to 0.09375
- shared_down: bfloat16 [1024, 4096], P(None, 'tp'), may hold values from -0.1875 to 0.1875
Outputs:
- mixed: bfloat16 [2048, 4096], P('sp', 'tp')
Inputs may be any that keep to these rules, and one draw needn't show every extreme that they name: `route_ids`: each row names 2 different experts. In each aligned block of 256 rows (the rows of one index of sp) no expert is named by more than 128 rows, a bound that some expert reaches in some blocks.
All inputs are finite; a program needn't handle non-finite values.
Results may differ from a plain program's by a relative error of at most 0.012.
Values may be sent and summed in bfloat16 or wider, within the bound.
A program may use at most 64 MiB of HBM per device.

v0:
```python
import jax
import jax.numpy as jnp
from jax import lax
from jax.sharding import PartitionSpec as P

D = 4096
CONV = 2048


norm_eps = 1e-06


def shifted(block, axis, distance):
    devices = range(lax.axis_size(axis))
    route = [(i - distance, i) for i in devices if i - distance in devices]
    return lax.ppermute(block, axis, route)


def shards(
    u_val,
    u_gate,
    conv_weight,
    conv_bias,
    ln_gain,
    ln_bias,
    proj_weight,
    resid,
    norm_gain,
    route_ids,
    route_wts,
    expert_gate,
    expert_up,
    expert_down,
    shared_gate,
    shared_up,
    shared_down,
):
    tok_rows = u_val.shape[0]
    sp_count = lax.axis_size("sp")
    tp_count = lax.axis_size("tp")
    kernel_width = conv_weight.shape[0]
    gated = (u_val.astype(jnp.float32) * jax.nn.sigmoid(u_gate.astype(jnp.float32))).astype(
        jnp.bfloat16
    )
    rim_rows = shifted(gated[tok_rows - (kernel_width - 1) :], "sp", 1)
    padded = lax.optimization_barrier(jnp.concatenate([rim_rows, gated], axis=0)).astype(
        jnp.float32
    )
    conv_sum = jnp.zeros((tok_rows, gated.shape[1]), jnp.float32) + conv_bias[None, :]
    for tap_index in range(kernel_width):
        conv_sum = (
            conv_sum + conv_weight[tap_index][None, :] * padded[tap_index : tap_index + tok_rows]
        )
    stat_sums = lax.psum((jnp.sum(conv_sum, axis=1), jnp.sum(conv_sum * conv_sum, axis=1)), "tp")
    channel_mean = stat_sums[0] / CONV
    channel_var = stat_sums[1] / CONV - channel_mean * channel_mean
    normed_conv = (conv_sum - channel_mean[:, None]) * lax.rsqrt(channel_var + norm_eps)[:, None]
    conv_out = jax.nn.silu(normed_conv * ln_gain + ln_bias).astype(jnp.bfloat16)
    projected = jnp.dot(
        lax.all_gather(conv_out, "tp", axis=1, tiled=True),
        proj_weight,
        preferred_element_type=jnp.float32,
    )
    residual_mid = (resid.astype(jnp.float32) + projected).astype(jnp.bfloat16)
    residual_wide = residual_mid.astype(jnp.float32)
    square_sum = lax.psum(jnp.sum(residual_wide * residual_wide, axis=1), "tp")
    normed_rows = (
        residual_wide * lax.rsqrt(square_sum / D + norm_eps)[:, None] * norm_gain
    ).astype(jnp.bfloat16)
    rows_full = lax.all_gather(normed_rows, "tp", axis=1, tiled=True)
    topk_count = route_ids.shape[1]
    capacity = 2 * tok_rows * topk_count // sp_count
    pair_ids = route_ids.reshape(-1)
    onehot = (pair_ids[:, None] == jnp.arange(sp_count, dtype=jnp.int32)[None, :]).astype(jnp.int32)
    before = jnp.cumsum(onehot, axis=0) - onehot
    position = jnp.sum(before * onehot, axis=1)
    pair_slot = pair_ids * capacity + position
    matches = (
        jnp.arange(sp_count * capacity, dtype=jnp.int32)[:, None] == pair_slot[None, :]
    ).astype(jnp.int32)
    pair_tok = jnp.arange(tok_rows * topk_count, dtype=jnp.int32) // topk_count
    filled = jnp.sum(matches, axis=1)
    slot_tok = jnp.sum(matches * pair_tok[None, :], axis=1) + (1 - filled) * tok_rows
    rows_ext = jnp.concatenate(
        [rows_full, jnp.zeros((1, rows_full.shape[1]), jnp.bfloat16)], axis=0
    )
    part_slots = capacity // tp_count
    tp_index = lax.axis_index("tp")
    local_slots = lax.dynamic_slice_in_dim(
        slot_tok.reshape(sp_count, capacity), tp_index * part_slots, part_slots, 1
    )
    send_rows = jnp.take(rows_ext, local_slots.reshape(-1), axis=0).reshape(
        sp_count, part_slots, -1
    )
    received = lax.all_to_all(send_rows, "sp", split_axis=0, concat_axis=0, tiled=True)
    arrived = lax.all_gather(received, "tp", axis=1, tiled=True)
    slot_rows = arrived.reshape(sp_count * capacity, -1)
    gate_pre = jnp.dot(slot_rows, expert_gate[0], preferred_element_type=jnp.float32)
    up_proj = jnp.dot(slot_rows, expert_up[0], preferred_element_type=jnp.float32)
    hidden = (jax.nn.silu(gate_pre) * up_proj).astype(jnp.bfloat16)
    shared_pre = jnp.dot(rows_full, shared_gate, preferred_element_type=jnp.float32)
    shared_upper = jnp.dot(rows_full, shared_up, preferred_element_type=jnp.float32)
    shared_hidden = (jax.nn.silu(shared_pre) * shared_upper).astype(jnp.bfloat16)
    out_cols = expert_down.shape[2]
    routed_rows = expert_down[0]
    routed_out = jnp.dot(
        lax.all_gather(hidden, "tp", axis=1, tiled=True),
        routed_rows,
        preferred_element_type=jnp.float32,
    )
    shared_out = jnp.dot(
        lax.all_gather(shared_hidden, "tp", axis=1, tiled=True),
        shared_down,
        preferred_element_type=jnp.float32,
    )
    expert_rows = routed_out.astype(jnp.bfloat16).reshape(sp_count, capacity, out_cols)
    returned_rows = lax.all_to_all(expert_rows, "sp", split_axis=0, concat_axis=0, tiled=True)
    returned_flat = returned_rows.reshape(sp_count * capacity, out_cols)
    picked = (
        jnp.take(returned_flat, pair_slot, axis=0)
        .astype(jnp.float32)
        .reshape(tok_rows, topk_count, out_cols)
    )
    routed = jnp.sum(picked * route_wts[:, :, None], axis=1)
    return (residual_wide + shared_out + routed).astype(jnp.bfloat16)


def solution(mesh):
    in_specs = (
        P("sp", "tp"),
        P("sp", "tp"),
        P(None, "tp"),
        P("tp"),
        P("tp"),
        P("tp"),
        P(None, "tp"),
        P("sp", "tp"),
        P("tp"),
        P("sp", None),
        P("sp", None),
        P("sp", None, "tp"),
        P("sp", None, "tp"),
        P("sp", None, "tp"),
        P(None, "tp"),
        P(None, "tp"),
        P(None, "tp"),
    )
    out_specs = P("sp", "tp")
    return jax.shard_map(shards, mesh=mesh, in_specs=in_specs, out_specs=out_specs, check_vma=False)
```

profile of v0, /device:TPU:1, one launch (start us, length us, event | category | flops | bytes accessed | tf_op | source)
XLA Modules:
  0.0 379.4 jit_solution(6599794522026167166)
XLA Ops:
  6.5 1.3 multiply_convert_fusion.1
  7.9 4.6 %collective-permute-start = (bf16[30,512]{1,0:T(8,128)(2,1)S(1)}, bf16[30,512]{1,0:T(8,128)(2,1)S(1)}, u32[]{:S(2)}, u32[]{:S(2)}) collective-permute-start(bf16[30,512]{1,0:T(8,128)(2,1)S(1)} %slice.264), channel_id=1, source_target_pairs={{0,4},{4,8},{8,12},{12,16},{16,20},{20,24},{24,28},{1,5},{5,9},{9,... | collective-permute-start | bytes 92168 | tf_op jit(solution)/shard_map/ppermute | solution.py:16
  12.5 1.2 fusion.61
  13.7 1.0 fusion.62
  14.7 0.0 collective-permute-done
  14.7 0.1 pad_maximum_fusion
  14.8 0.1 convert_element_type.57
  14.8 0.0 copy-done.7
  14.8 0.0 copy-start.8
  14.9 0.0 copy-start.9
  14.9 0.0 copy-start.14
  14.9 2.6 fusion.59
  17.5 8.2 %all-reduce.1 = (f32[256]{0:T(256)S(1)}, f32[256]{0:T(256)S(1)}) all-reduce(f32[256]{0:T(256)S(1)} %get-tuple-element.6, f32[256]{0:T(256)S(1)} %get-tuple-element.5), channel_id=1, replica_groups=mesh['sp'=8,'tp'=4] {'tp'}, use_global_device_ids=true, to_apply=%region_3.0 | all-reduce | flops 512 | bytes 4096 | tf_op jit(solution)/shard_map/psum | solution.py:54
  25.7 1.0 multiply_convert_fusion
  26.7 0.0 all-gather.5.cloned.1.call-update
  26.7 0.0 copy-start.6
  26.7 0.0 copy-start.5
  26.7 0.0 all-gather.7.cloned.1.call-start
  26.8 26.6 %all-gather.5.cloned.1.call-done = bf16[256,2048]{1,0:T(8,128)(2,1)} async-done(((bf16[256,512]{1,0:T(8,128)(2,1)}), bf16[256,2048]{1,0:T(8,128)(2,1)}) %all-gather.5.cloned.1.call-update) | async-done | bytes 1048592 | tf_op jit(solution)/shard_map/all_gather | solution.py:60
  53.4 3.9 %fusion.19 = (f32[256]{0:T(256)S(1)}, bf16[256,1024]{1,0:T(8,128)(2,1)S(1)}) fusion(bf16[256,2048]{1,0:T(8,128)(2,1)} %all-gather.5.cloned.1.call-done, bf16[2048,1024]{1,0:T(8,128)(2,1)} %param.23, bf16[256,1024]{1,0:T(8,128)(2,1)S(1)} %copy-done.14), kind=kOutput, calls=%fused_computation.26 | convolution fusion | flops 1075314432 | bytes 6292480 | tf_op jit(solution)/shard_map/dot_general | solution.py:59
  57.3 6.9 %psum.23 = f32[256]{0:T(256)S(1)} all-reduce(f32[256]{0:T(256)S(1)} %get-tuple-element.47), channel_id=1, replica_groups=mesh['sp'=8,'tp'=4] {'tp'}, use_global_device_ids=true, to_apply=%region_5.6 | all-reduce | flops 256 | bytes 2048 | tf_op jit(solution)/shard_map/psum | solution.py:66
  64.2 1.0 fusion.21
  65.2 0.0 all-gather.7.cloned.1.call-update
  65.3 0.0 all-gather.9.cloned.1.call-start
  65.3 0.1 copy.28
  65.5 0.1 reshape.151
  65.6 0.1 eq.39
  65.8 1.1 reduce-window.6
  66.9 0.2 slice_reduce_fusion
  67.2 0.1 fusion.54
  67.3 0.6 convert_reduce_fusion
  67.9 0.1 compare_and_fusion
  68.0 0.1 reshape.153
  68.1 34.5 %all-gather.7.cloned.1.call-done = bf16[256,4096]{1,0:T(8,128)(2,1)} async-done(((bf16[256,1024]{1,0:T(8,128)(2,1)}), bf16[256,4096]{1,0:T(8,128)(2,1)}) %all-gather.7.cloned.1.call-update) | async-done | bytes 2097168 | tf_op jit(solution)/shard_map/all_gather | solution.py:70
  102.6 3.2 concatenate.7
  105.9 7.1 %gather_fusion = bf16[256,4096]{1,0:T(8,128)(2,1)} fusion(bf16[257,4096]{1,0:T(8,128)(2,1)} %concatenate.7, s32[1024]{0:T(1024)S(1)} %pad_clamp_fusion.1), kind=kCustom, calls=%fused_computation | custom fusion | bytes 4195328 | tf_op jit(solution)/shard_map/jit(_take)/gather | solution.py:92
  112.9 1.8 broadcast_select_fusion
  114.8 53.3 %all_to_all.10 = bf16[8,32,4096]{2,1,0:T(8,128)(2,1)} all-to-all(bf16[8,32,4096]{2,1,0:T(8,128)(2,1)S(1)} %broadcast_select_fusion), channel_id=1, replica_groups=mesh['sp'=8,'tp'=4] {'sp'}, dimensions={0} | all-to-all | bytes 4194304 | tf_op jit(solution)/shard_map/all_to_all | solution.py:95
  168.1 0.0 all-gather.9.cloned.1.call-update
  168.2 0.2 all-gather.11.cloned.1.call-start
  168.4 85.6 %all-gather.9.cloned.1.call-done = bf16[8,128,4096]{2,1,0:T(8,128)(2,1)} async-done(((bf16[8,32,4096]{2,1,0:T(8,128)(2,1)}), bf16[8,128,4096]{2,1,0:T(8,128)(2,1)}) %all-gather.9.cloned.1.call-update) | async-done | bytes 8388624 | tf_op jit(solution)/shard_map/all_gather | solution.py:96
  254.0 6.5 %fusion.4 = f32[1024,256]{1,0:T(8,128)S(1)} fusion(bf16[1024,4096]{1,0:T(8,128)(2,1)} %bitcast.110, bf16[1,4096,256]{2,1,0:T(8,128)(2,1)} %param.28), kind=kOutput, calls=%fused_computation.6 | convolution fusion | flops 2147483648 | bytes 11534336 | tf_op jit(solution)/shard_map/dot_general | solution.py:98
  260.4 0.5 copy-done.12
  260.9 3.2 fusion.14
  264.1 0.0 all-gather.11.cloned.1.call-update
  264.1 35.2 %all-gather.11.cloned.1.call-done = bf16[1024,1024]{1,0:T(8,128)(2,1)} async-done(((bf16[1024,256]{1,0:T(8,128)(2,1)}), bf16[1024,1024]{1,0:T(8,128)(2,1)}) %all-gather.11.cloned.1.call-update) | async-done | bytes 2097168 | tf_op jit(solution)/shard_map/all_gather | solution.py:107
  299.3 5.3 %fusion.6 = bf16[1024,1024]{1,0:T(8,128)(2,1)} fusion(bf16[1024,1024]{1,0:T(8,128)(2,1)} %all-gather.11.cloned.1.call-done, bf16[1,1024,1024]{2,1,0:T(8,128)(2,1)S(1)} %copy-done), kind=kOutput, calls=%fused_computation.14 | convolution fusion | flops 2148532224 | bytes 6291456 | tf_op jit(solution)/shard_map/dot_general | solution.py:106
  304.5 5.6 %all-to-all-start.1 = ((bf16[8,128,1024]{2,1,0:T(8,128)(2,1)}), bf16[8,128,1024]{2,1,0:T(8,128)(2,1)}, u32[]{:S(2)}, u32[]{:S(2)}) async-start(bf16[8,128,1024]{2,1,0:T(8,128)(2,1)} %bitcast.75), calls=%async_computation.1 | async-start | bytes 4194304 | tf_op jit(solution)/shard_map/all_to_all | solution.py:117
  310.1 0.1 reduce_sum.71
  310.3 0.1 copy.32
  310.4 0.1 mul.549
  310.6 0.1 copy.30
  310.7 0.2 copy.31
  310.9 0.1 copy.33
  311.0 0.0 copy-start.13
  311.0 3.1 fusion.63
  314.1 0.4 copy-done.13
  314.5 0.7 fusion.18
  315.2 14.2 %all_gather.17 = bf16[256,1024]{1,0:T(8,128)(2,1)} all-gather(bf16[256,256]{1,0:T(8,128)(2,1)S(1)} %fusion.18), channel_id=1, replica_groups=mesh['sp'=8,'tp'=4] {'tp'}, dimensions={1}, use_global_device_ids=true | all-gather | bytes 655360 | tf_op jit(solution)/shard_map/all_gather | solution.py:112
  329.4 28.9 %all-to-all-done.1 = bf16[8,128,1024]{2,1,0:T(8,128)(2,1)} async-done(((bf16[8,128,1024]{2,1,0:T(8,128)(2,1)}), bf16[8,128,1024]{2,1,0:T(8,128)(2,1)}, u32[]{:S(2)}, u32[]{:S(2)}) %all-to-all-start.1) | async-done | bytes 2097184 | tf_op jit(solution)/shard_map/all_to_all | solution.py:117
  358.3 4.6 %gather_fusion.1 = bf16[512,1024]{1,0:T(8,128)(2,1)S(1)} fusion(bf16[1024,1024]{1,0:T(8,128)(2,1)} %bitcast.41, s32[1024]{0:T(1024)S(1)} %pad_clamp_fusion), kind=kCustom, calls=%fused_computation.1 | custom fusion | bytes 2099200 | tf_op jit(solution)/shard_map/jit(_take)/gather | solution.py:120
  362.9 1.2 gather.15
  364.1 5.6 %multiply_reduce_fusion = f32[256,1024]{1,0:T(8,128)S(1)} fusion(bf16[256,2,1024]{2,1,0:T(2,128)(2,1)} %gather.15, pred[256,2]{1,0:T(8,128)(4,1)S(1)} %copy.31, f32[256,2]{1,0:T(8,128)S(1)} %copy.33), kind=kLoop, calls=%fused_computation.8 | loop fusion | flops 1835008 | bytes 2099712 | tf_op jit(solution)/shard_map/reduce_sum | solution.py:124
  369.8 3.1 fusion.17
  (36 shorter events, 0.2 us)
Async XLA Ops:
  6.5 292.8 %copy-start = (bf16[1,1024,1024]{2,1,0:T(8,128)(2,1)S(1)}, bf16[1,1024,1024]{2,1,0:T(8,128)(2,1)}, u32[]{:S(2)}) copy-start(bf16[1,1024,1024]{2,1,0:T(8,128)(2,1)} %param.30) | copy-start | bytes 6291460
  6.5 8.3 %copy-start.7 = (f32[512]{0:T(512)S(1)}, f32[512]{0:T(512)}, u32[]{:S(2)}) copy-start(f32[512]{0:T(512)} %param.20) | copy-start | bytes 6148
  6.5 46.9 %all-gather.5.cloned.1.call-start = ((), (), s32[]{:S(2)}) async-start(), calls=%async_computation.2 | async-start | bytes 1310720 | tf_op jit(solution)/shard_map/all_gather | solution.py:60
  7.9 6.8 %collective-permute-start = (bf16[30,512]{1,0:T(8,128)(2,1)S(1)}, bf16[30,512]{1,0:T(8,128)(2,1)S(1)}, u32[]{:S(2)}, u32[]{:S(2)}) collective-permute-start(bf16[30,512]{1,0:T(8,128)(2,1)S(1)} %slice.264), channel_id=1, source_target_pairs={{0,4},{4,8},{8,12},{12,16},{16,20},{20,24},{24,28},{1,5},{5,9},{9,... | collective-permute-start | bytes 92168 | tf_op jit(solution)/shard_map/ppermute | solution.py:16
  14.8 10.9 %copy-start.8 = (f32[512]{0:T(512)S(1)}, f32[512]{0:T(512)}, u32[]{:S(2)}) copy-start(f32[512]{0:T(512)} %param.22) | copy-start | bytes 6148
  14.9 10.9 %copy-start.9 = (f32[512]{0:T(512)S(1)}, f32[512]{0:T(512)}, u32[]{:S(2)}) copy-start(f32[512]{0:T(512)} %param.21) | copy-start | bytes 6148
  14.9 38.6 %copy-start.14 = (bf16[256,1024]{1,0:T(8,128)(2,1)S(1)}, bf16[256,1024]{1,0:T(8,128)(2,1)}, u32[]{:S(2)}) copy-start(bf16[256,1024]{1,0:T(8,128)(2,1)} %param.24) | copy-start | bytes 1572868
  26.7 37.5 %copy-start.6 = (f32[1024]{0:T(1024)S(1)}, f32[1024]{0:T(1024)}, u32[]{:S(2)}) copy-start(f32[1024]{0:T(1024)} %param.25) | copy-start | bytes 12292
  26.7 38.6 %copy-start.5 = (s32[256,2]{0,1:T(2,128)S(1)}, s32[256,2]{0,1:T(2,128)}, u32[]{:S(2)}) copy-start(s32[256,2]{0,1:T(2,128)} %param.26) | copy-start | bytes 6148
  26.7 75.9 %all-gather.7.cloned.1.call-start = ((), (), s32[]{:S(2)}) async-start(), calls=%async_computation.3 | async-start | bytes 2621440 | tf_op jit(solution)/shard_map/all_gather | solution.py:70
  57.3 48.6 %copy-start.2 = (bf16[256,1024]{1,0:T(8,128)(2,1)}, bf16[256,1024]{1,0:T(8,128)(2,1)S(1)}, u32[]{:S(2)}) copy-start(bf16[256,1024]{1,0:T(8,128)(2,1)S(1)} %get-tuple-element.48) | copy-start | bytes 1572868
  65.3 188.7 %all-gather.9.cloned.1.call-start = ((), (), s32[]{:S(2)}) async-start(), calls=%async_computation.4 | async-start | bytes 10485760 | tf_op jit(solution)/shard_map/all_gather | solution.py:96
  168.2 131.1 %all-gather.11.cloned.1.call-start = ((), (), s32[]{:S(2)}) async-start(), calls=%async_computation.5 | async-start | bytes 2621440 | tf_op jit(solution)/shard_map/all_gather | solution.py:107
  254.0 6.5 %copy-start.11 = (bf16[8,128,4096]{2,1,0:T(8,128)(2,1)S(1)}, bf16[8,128,4096]{2,1,0:T(8,128)(2,1)}, u32[]{:S(2)}) copy-start(bf16[8,128,4096]{2,1,0:T(8,128)(2,1)} %all-gather.9.cloned.1.call-done) | copy-start | bytes 25165828
  254.0 7.0 %copy-start.12 = (bf16[1,4096,256]{2,1,0:T(8,128)(2,1)S(1)}, bf16[1,4096,256]{2,1,0:T(8,128)(2,1)}, u32[]{:S(2)}) copy-start(bf16[1,4096,256]{2,1,0:T(8,128)(2,1)} %param.29) | copy-start | bytes 6291460
  304.5 6.3 %copy-start.10 = (f32[256,2]{0,1:T(2,128)S(1)}, f32[256,2]{0,1:T(2,128)}, u32[]{:S(2)}) copy-start(f32[256,2]{0,1:T(2,128)} %param.27) | copy-start | bytes 6148
  304.5 53.7 %all-to-all-start.1 = ((bf16[8,128,1024]{2,1,0:T(8,128)(2,1)}), bf16[8,128,1024]{2,1,0:T(8,128)(2,1)}, u32[]{:S(2)}, u32[]{:S(2)}) async-start(bf16[8,128,1024]{2,1,0:T(8,128)(2,1)} %bitcast.75), calls=%async_computation.1 | async-start | bytes 4194304 | tf_op jit(solution)/shard_map/all_to_all | solution.py:117
  311.0 3.1 copy-start.1
  311.0 3.5 copy-start.13
  364.1 5.6 %copy-start.3 = (bf16[256,1024]{1,0:T(8,128)(2,1)S(1)}, bf16[256,1024]{1,0:T(8,128)(2,1)}, u32[]{:S(2)}) copy-start(bf16[256,1024]{1,0:T(8,128)(2,1)} %copy-done.2) | copy-start | bytes 1572868
  364.1 5.6 %copy-start.4 = (bf16[256,1024]{1,0:T(8,128)(2,1)S(1)}, bf16[256,1024]{1,0:T(8,128)(2,1)}, u32[]{:S(2)}) copy-start(bf16[256,1024]{1,0:T(8,128)(2,1)} %all_gather.17) | copy-start | bytes 1572868
Sparse Core Ops, SparseCore 0:
  26.8 26.5 all-gather.4
  65.4 37.2 all-gather.6
  168.3 85.6 all-gather.8
  264.2 35.0 all-gather.10
where the time goes:
time: 381 us; the launch traced here: 379 us
  waiting for transfers between devices  211 us (55%)
  blocking collectives  82.7 us (22%)
  matrix products  25.7 us (7%)
  local copies, waits for them, and re-layouts  20.7 us (5%)
  other arithmetic  15.6 us (4%)
  between operations  13.5 us (4%)
  starting transfers between devices  10.5 us (3%)
    all_gather x1, waiting for transfers between devices, shards(): arrived = lax.all_gather(received, 'tp', axis=1, tiled=True)  85.6 us
    all_to_all x1, blocking collectives, shards(): lax.all_to_all(send_rows, 'sp', split_axis=0, concat_axis=0, tiled=True)  53.3 us
    all_gather x1, waiting for transfers between devices, shards(): lax.all_gather(hidden, 'tp', axis=1, tiled=True)  35.2 us
    all_gather x1, waiting for transfers between devices, shards(): rows_full = lax.all_gather(normed_rows, 'tp', axis=1, tiled=True)  34.5 us
    all_to_all x1, waiting for transfers between devices, shards(): lax.all_to_all(expert_rows, 'sp', split_axis=0, concat_axis=0, tiled=True)  28.9 us
    all_gather x1, waiting for transfers between devices, shards(): lax.all_gather(conv_out, 'tp', axis=1, tiled=True)  26.6 us
    all_gather x1, blocking collectives, shards(): lax.all_gather(shared_hidden, 'tp', axis=1, tiled=True)  14.2 us
    psum x1, blocking collectives, shards(): lax.psum((jnp.sum(conv_sum, axis=1), jnp.sum(conv_sum * conv_sum, axis=1)...  8.19 us
  transfers between devices with their start and end apart: 6, of which 5 were waited for; matrix products, arithmetic and copies ran while one was open for 3% of the time, Pallas kernels for 0%

commit v1 on v0

--- a/solution.py
+++ b/solution.py
@@ -1,6 +1,10 @@
+import functools
+
 import jax
 import jax.numpy as jnp
 from jax import lax
+from jax.experimental import pallas as pl
+from jax.experimental.pallas import tpu as pltpu
 from jax.sharding import PartitionSpec as P
 
 D = 4096
@@ -125,6 +129,477 @@
     return (residual_wide + shared_out + routed).astype(jnp.bfloat16)
 
 
+VMEM = pltpu.VMEM
+DMA = pltpu.SemaphoreType.DMA
+F32 = jnp.float32
+BF16 = jnp.bfloat16
+
+
+def rcopy(src, dst, send_sem, recv_sem, device):
+    return pltpu.make_async_remote_copy(
+        src_ref=src,
+        dst_ref=dst,
+        send_sem=send_sem,
+        recv_sem=recv_sem,
+        device_id=device,
+        device_id_type=pl.DeviceIdType.MESH,
+    )
+
+
+def dot(a, b):
+    return jnp.dot(a, b, preferred_element_type=F32)
+
+
+def greet(nsp, ntp, me, t):
+    barrier = pltpu.get_barrier_semaphore()
+    for j in range(1, ntp):
+        pl.semaphore_signal(
+            barrier, inc=1, device_id=(me, (t + j) % ntp), device_id_type=pl.DeviceIdType.MESH
+        )
+    for j in range(1, nsp):
+        pl.semaphore_signal(
+            barrier, inc=1, device_id=((me + j) % nsp, t), device_id_type=pl.DeviceIdType.MESH
+        )
+    pl.semaphore_wait(barrier, ntp - 1 + nsp - 1)
+
+
+def front_kernel(
+    nsp, ntp,
+    conv, gain, bias, resid, ngain, route, proj_hbm,
+    normed, mid, route_all,
+    proj, gbuf, st, st2, rbuf,
+    lsem, gsend, grecv, ssend, srecv, s2send, s2recv, rsend, rrecv,
+):
+    me = lax.axis_index("sp")
+    t = lax.axis_index("tp")
+    tok = conv.shape[0]
+    weights = pltpu.make_async_copy(proj_hbm, proj, lsem.at[0])
+    weights.start()
+    greet(nsp, ntp, me, t)
+    tables = []
+    for j in range(1, nsp):
+        e = (me + j) % nsp
+        copy = rcopy(route.at[e], rbuf.at[me], rsend.at[j - 1], rrecv.at[j - 1], (e, t))
+        copy.start()
+        tables.append(copy)
+    rbuf[me] = route[me]
+
+    def exchange(stat, columns, send, recv):
+        lane = lax.broadcasted_iota(jnp.int32, (tok, 128), 1)
+        packed = jnp.zeros((tok, 128), F32)
+        for i, column in enumerate(columns):
+            packed = packed + jnp.where(lane == i, column, 0.0)
+        stat[t] = jnp.transpose(packed)[0:8, :]
+        copies = []
+        for j in range(1, ntp):
+            copy = rcopy(
+                stat.at[t], stat.at[t], send.at[j - 1], recv.at[j - 1], (me, (t + j) % ntp)
+            )
+            copy.start()
+            copies.append(copy)
+        for copy in copies:
+            copy.wait()
+        total = stat[0]
+        for i in range(1, ntp):
+            total = total + stat[i]
+        return jnp.transpose(jnp.concatenate([total] * 16, axis=0))
+
+    x = conv[...]
+    sums = exchange(
+        st,
+        [jnp.sum(x, axis=1, keepdims=True), jnp.sum(x * x, axis=1, keepdims=True)],
+        ssend,
+        srecv,
+    )
+    channels = conv.shape[1] * ntp
+    mean = sums[:, 0:1] / channels
+    var = sums[:, 1:2] / channels - mean * mean
+    v = (x - mean) * lax.rsqrt(var + norm_eps) * gain[...] + bias[...]
+    gbuf[t] = (v / (1.0 + jnp.exp(-v))).astype(BF16)
+    copies = []
+    for j in range(1, ntp):
+        copy = rcopy(gbuf.at[t], gbuf.at[t], gsend.at[j - 1], grecv.at[j - 1], (me, (t + j) % ntp))
+        copy.start()
+        copies.append(copy)
+    weights.wait()
+    total = resid[...].astype(F32) + dot(gbuf[t], proj[t])
+    for j in range(1, ntp):
+        copies[j - 1].wait_recv()
+        q = (t - j + ntp) % ntp
+        total = total + dot(gbuf[q], proj[q])
+    mid[...] = total.astype(BF16)
+    wide = mid[...].astype(F32)
+    squares = exchange(st2, [jnp.sum(wide * wide, axis=1, keepdims=True)], s2send, s2recv)
+    scale = lax.rsqrt(squares[:, 0:1] / (mid.shape[1] * ntp) + norm_eps)
+    normed[...] = (wide * scale * ngain[...]).astype(BF16)
+    for copy in copies:
+        copy.wait_send()
+    for copy in tables:
+        copy.wait()
+    route_all[...] = rbuf[...]
+
+
+def expert_kernel(
+    nsp, ntp, cap,
+    normed, mid, route, poscol, wg_h, wu_h, sg_h, su_h, wd_h, sd_h,
+    out,
+    buf, wg, wu, sg, su, wd, sd, acc, hid, shid, osend, ret,
+    lsem, recv, zsend, xsend, ysend, relay, dsend, hsend, hrecv, shsend, shrecv, osem, orecv,
+):
+    me = lax.axis_index("sp")
+    t = lax.axis_index("tp")
+    tok, width = normed.shape
+    half = tok // 2
+    hidden_width = wg.shape[2]
+    nz = nsp // 2
+    z = me // 2
+    c = me % 2
+    partner = me + 1 - 2 * c
+    t1 = t + 1 - 2 * (t % 2)
+    t2 = t + 2 - 4 * (t // 2)
+    t3 = 3 - t
+    loads = [
+        pltpu.make_async_copy(a, b, lsem.at[i])
+        for i, (a, b) in enumerate(
+            [(wg_h, wg), (wu_h, wu), (sg_h, sg), (su_h, su), (wd_h, wd), (sd_h, sd)]
+        )
+    ]
+    own = pltpu.make_async_copy(normed, buf.at[me, t], lsem.at[6])
+    own.start()
+    for load in loads:
+        load.start()
+    greet(nsp, ntp, me, t)
+    own.wait()
+
+    def rows(b, q, h):
+        return buf.at[b, q, pl.ds(h * half, half)]
+
+    def push(b, q, h, sem, device):
+        return rcopy(rows(b, q, h), rows(b, q, h), sem, recv.at[b, q, h], device)
+
+    def arrived(b, q, h):
+        push(b, q, h, zsend.at[0, 0], (me, t1)).wait_recv()
+
+    def spread(k, b):
+        copies = []
+        for h in range(2):
+            copies.append(push(b, t, h, xsend.at[k, h], (me, t1)))
+            copies.append(push(b, t, h, ysend.at[k, h], (me, t2)))
+            copies.append(push(b, t, h, dsend.at[k, 0, h], (partner, t)))
+        return copies
+
+    def relays(k, b):
+        return [
+            push(b, t1, 0, relay.at[k, 0], (me, t2)),
+            push(b, t2, 1, relay.at[k, 1], (me, t1)),
+        ]
+
+    def across(k, b, i, q, h):
+        return push(b, q, h, dsend.at[k, i, h], (partner, t))
+
+    far = []
+    for k in range(1, nz):
+        for h in range(2):
+            far.append(push(me, t, h, zsend.at[k - 1, h], (2 * ((z + k) % nz) + c, t)))
+    for copy in far:
+        copy.start()
+    for copy in spread(0, me):
+        copy.start()
+    for load in loads:
+        load.wait()
+
+    def gate_up(i, b, q, first):
+        data = buf[b, q]
+        g = dot(data, wg[q])
+        u = dot(data, wu[q])
+        if first:
+            acc[i, 0] = g
+            acc[i, 1] = u
+        else:
+            acc[i, 0] += g
+            acc[i, 1] += u
+
+    def selection(b):
+        slot = lax.broadcasted_iota(jnp.int32, (cap, tok), 0).astype(F32)
+        return jnp.where(slot == route[b, 0:1, :], 1.0, 0.0)
+
+    def hidden_copies(b):
+        return [
+            rcopy(hid.at[b, t], hid.at[b, t], hsend.at[b, j - 1], hrecv.at[b, j - 1],
+                  (me, (t + j) % ntp))
+            for j in range(1, ntp)
+        ]
+
+    def shared_copies():
+        return [
+            rcopy(shid.at[t], shid.at[t], shsend.at[j - 1], shrecv.at[j - 1], (me, (t + j) % ntp))
+            for j in range(1, ntp)
+        ]
+
+    def gated(g, u):
+        return (g / (1.0 + jnp.exp(-g)) * u).astype(BF16)
+
+    def finish(i, b):
+        hs = dot(selection(b).astype(BF16), gated(acc[i, 0], acc[i, 1]))
+        hid[b, t] = hs.astype(BF16)
+        for copy in hidden_copies(b):
+            copy.start()
+
+    def home(b):
+        return rcopy(osend.at[b], ret.at[me], osem.at[b], orecv.at[me], (b, t))
+
+    def down(b):
+        for j in range(1, ntp):
+            q = (t - j + ntp) % ntp
+            rcopy(hid.at[b, q], hid.at[b, q], hsend.at[b, j - 1], hrecv.at[b, j - 1],
+                  (me, t1)).wait_recv()
+        o = dot(hid[b, 0], wd[0])
+        for q in range(1, ntp):
+            o = o + dot(hid[b, q], wd[q])
+        weight = jnp.sum(selection(b) * route[b, 1:2, :], axis=1, keepdims=True)
+        return (o * weight).astype(BF16)
+
+    def step(k, carry):
+        zk = (z - k + nz) % nz
+
+        @pl.when(k < nz)
+        def _():
+            b = 2 * zk + c
+            pb = 2 * zk + 1 - c
+            forward = relays(k, b)
+            for h in range(2):
+                arrived(b, t1, h)
+                if h == 0:
+                    forward[0].start()
+                across(k, b, 1, t1, h).start()
+            for h in range(2):
+                arrived(b, t2, h)
+                if h == 1:
+                    forward[1].start()
+                across(k, b, 2, t2, h).start()
+
+            @pl.when(k < nz - 1)
+            def _():
+                bn = 2 * ((z - k - 1 + nz) % nz) + c
+                for h in range(2):
+                    arrived(bn, t, h)
+                for copy in spread(k + 1, bn):
+                    copy.start()
+
+            gate_up(0, b, t, True)
+            gate_up(0, b, t1, False)
+            gate_up(0, b, t2, False)
+            for i, q in enumerate((t, t1, t2)):
+                for h in range(2):
+                    arrived(pb, q, h)
+                gate_up(1, pb, q, i == 0)
+            for h in range(2):
+                arrived(b, t3, h)
+                across(k, b, 3, t3, h).start()
+            gate_up(0, b, t3, False)
+            finish(0, b)
+            for h in range(2):
+                arrived(pb, t3, h)
+            gate_up(1, pb, t3, False)
+            finish(1, pb)
+
+        @pl.when(k == 0)
+        def _():
+            def quarter(q, state):
+                data = buf[me, q]
+                g = dot(data, sg[q])
+                u = dot(data, su[q])
+                acc[0, 0] = jnp.where(q == 0, g, acc[0, 0] + g)
+                acc[0, 1] = jnp.where(q == 0, u, acc[0, 1] + u)
+                return state
+
+            lax.fori_loop(0, ntp, quarter, 0)
+            shid[t] = gated(acc[0, 0], acc[0, 1])
+            for copy in shared_copies():
+                copy.start()
+
+        @pl.when(k == 1)
+        def _():
+            ret[me] = down(me)
+            osend[partner] = down(partner)
+            home(partner).start()
+
+        @pl.when(k > 1)
+        def _():
+            zp = (z - k + 1 + nz) % nz
+
+            def one(i, state):
+                b = 2 * zp + i
+                osend[b] = down(b)
+                home(b).start()
+                return state
+
+            lax.fori_loop(0, 2, one, 0)
+
+        return carry
+
+    lax.fori_loop(0, nz + 1, step, 0)
+
+    for copy in shared_copies():
+        copy.wait_send()
+    for j in range(1, ntp):
+        q = (t - j + ntp) % ntp
+        rcopy(shid.at[q], shid.at[q], shsend.at[j - 1], shrecv.at[j - 1], (me, t1)).wait_recv()
+    total = mid[...].astype(F32)
+    for q in range(ntp):
+        total = total + dot(shid[q], sd[q])
+
+    def drain(k, carry):
+        b = 2 * ((z - k + nz) % nz) + c
+        for copy in spread(k, b) + relays(k, b):
+            copy.wait_send()
+        for i, q in ((1, t1), (2, t2), (3, t3)):
+            for h in range(2):
+                across(k, b, i, q, h).wait_send()
+        return carry
+
+    lax.fori_loop(0, nz, drain, 0)
+    for copy in far:
+        copy.wait_send()
+
+    def drain_hidden(b, carry):
+        for copy in hidden_copies(b):
+            copy.wait_send()
+        return carry
+
+    lax.fori_loop(0, nsp, drain_hidden, 0)
+    for j in range(1, nsp):
+        e = (me + j) % nsp
+        rcopy(osend.at[e], ret.at[e], osem.at[e], orecv.at[e], (e, t)).wait()
+    lane = lax.broadcasted_iota(jnp.int32, (tok, cap), 1).astype(F32)
+    for e in range(nsp):
+        pick = jnp.where(lane == poscol[:, e : e + 1], 1.0, 0.0).astype(BF16)
+        total = total + dot(pick, ret[e])
+    out[...] = total.astype(BF16)
+
+
+def fast_shards(
+    u_val, u_gate, conv_weight, conv_bias, ln_gain, ln_bias, proj_weight, resid, norm_gain,
+    route_ids, route_wts, expert_gate, expert_up, expert_down, shared_gate, shared_up, shared_down,
+):
+    tok = u_val.shape[0]
+    nsp = lax.axis_size("sp")
+    ntp = lax.axis_size("tp")
+    taps = conv_weight.shape[0]
+    gated = (u_val.astype(F32) * jax.nn.sigmoid(u_gate.astype(F32))).astype(BF16)
+    rim = shifted(gated[tok - (taps - 1) :], "sp", 1)
+    padded = lax.optimization_barrier(jnp.concatenate([rim, gated], axis=0)).astype(F32)
+    conv_sum = jnp.zeros((tok, gated.shape[1]), F32) + conv_bias[None, :]
+    for i in range(taps):
+        conv_sum = conv_sum + conv_weight[i][None, :] * padded[i : i + tok]
+
+    top = route_ids.shape[1]
+    cap = 2 * tok * top // nsp
+    experts = jnp.arange(nsp, dtype=jnp.int32)
+    named = jnp.zeros((nsp, tok), F32)
+    weight = jnp.zeros((nsp, tok), F32)
+    for k in range(top):
+        hit = route_ids[:, k][None, :] == experts[:, None]
+        named = named + hit.astype(F32)
+        weight = weight + jnp.where(hit, route_wts[:, k][None, :], 0.0)
+    earlier = (jnp.arange(tok)[:, None] < jnp.arange(tok)[None, :]).astype(BF16)
+    pos = jnp.where(named > 0, dot(named.astype(BF16), earlier), -1.0)
+    table = jnp.concatenate(
+        [pos[:, None, :], weight[:, None, :], jnp.zeros((nsp, 6, tok), F32)], axis=1
+    )
+    poscol = jnp.concatenate([pos.T, jnp.full((tok, 128 - nsp), -1.0, F32)], axis=1)
+
+    ch = conv_sum.shape[1]
+    width = resid.shape[1]
+    vm = pl.BlockSpec(memory_space=VMEM)
+    hbm = pl.BlockSpec(memory_space=pl.ANY)
+    normed, mid, route_all = pl.pallas_call(
+        functools.partial(front_kernel, nsp, ntp),
+        out_shape=[
+            jax.ShapeDtypeStruct((tok, width), BF16),
+            jax.ShapeDtypeStruct((tok, width), BF16),
+            jax.ShapeDtypeStruct((nsp, 8, tok), F32),
+        ],
+        in_specs=[vm] * 6 + [hbm],
+        out_specs=[vm] * 3,
+        scratch_shapes=[
+            VMEM((ntp, ch, width), BF16),
+            VMEM((ntp, tok, ch), BF16),
+            VMEM((ntp, 8, tok), F32),
+            VMEM((ntp, 8, tok), F32),
+            VMEM((nsp, 8, tok), F32),
+            DMA((1,)),
+            DMA((ntp - 1,)), DMA((ntp - 1,)),
+            DMA((ntp - 1,)), DMA((ntp - 1,)),
+            DMA((ntp - 1,)), DMA((ntp - 1,)),
+            DMA((nsp - 1,)), DMA((nsp - 1,)),
+        ],
+        compiler_params=pltpu.CompilerParams(
+            collective_id=1, has_side_effects=True, vmem_limit_bytes=24 << 20
+        ),
+        name="front",
+    )(
+        conv_sum, ln_gain[None, :], ln_bias[None, :], resid, norm_gain[None, :], table,
+        proj_weight.reshape(ntp, ch, width),
+    )
+
+    hw = expert_gate.shape[2]
+    sw = shared_gate.shape[1]
+    nz = nsp // 2
+    return pl.pallas_call(
+        functools.partial(expert_kernel, nsp, ntp, cap),
+        out_shape=jax.ShapeDtypeStruct((tok, width), BF16),
+        in_specs=[vm] * 4 + [hbm] * 6,
+        out_specs=vm,
+        scratch_shapes=[
+            VMEM((nsp, ntp, tok, width), BF16),
+            VMEM((ntp, width, hw), BF16),
+            VMEM((ntp, width, hw), BF16),
+            VMEM((ntp, width, sw), BF16),
+            VMEM((ntp, width, sw), BF16),
+            VMEM((ntp, hw, width), BF16),
+            VMEM((ntp, sw, width), BF16),
+            VMEM((2, 2, tok, hw), F32),
+            VMEM((nsp, ntp, cap, hw), BF16),
+            VMEM((ntp, tok, sw), BF16),
+            VMEM((nsp, cap, width), BF16),
+            VMEM((nsp, cap, width), BF16),
+            DMA((7,)),
+            DMA((nsp, ntp, 2)),
+            DMA((nz - 1, 2)),
+            DMA((nz, 2)), DMA((nz, 2)), DMA((nz, 2)),
+            DMA((nz, ntp, 2)),
+            DMA((nsp, ntp - 1)), DMA((nsp, ntp - 1)),
+            DMA((ntp - 1,)), DMA((ntp - 1,)),
+            DMA((nsp,)), DMA((nsp,)),
+        ],
+        compiler_params=pltpu.CompilerParams(
+            collective_id=2, has_side_effects=True, vmem_limit_bytes=56 << 20
+        ),
+        name="experts",
+    )(
+        normed, mid, route_all, poscol,
+        expert_gate[0].reshape(ntp, width, hw),
+        expert_up[0].reshape(ntp, width, hw),
+        shared_gate.reshape(ntp, width, sw),
+        shared_up.reshape(ntp, width, sw),
+        expert_down[0].reshape(ntp, hw, width),
+        shared_down.reshape(ntp, sw, width),
+    )
+
+
+def chosen(*args):
+    tok, width = args[7].shape
+    nsp = lax.axis_size("sp")
+    ntp = lax.axis_size("tp")
+    cap = 2 * tok * args[9].shape[1] // nsp
+    fits = 2 * nsp * ntp * tok * width <= 16 << 20
+    aligned = tok % 256 == 0 and width % 128 == 0 and cap % 128 == 0
+    if ntp == 4 and nsp % 2 == 0 and fits and aligned:
+        return fast_shards(*args)
+    return shards(*args)
+
+
 def solution(mesh):
     in_specs = (
         P("sp", "tp"),
@@ -146,4 +621,4 @@
         P(None, "tp"),
     )
     out_specs = P("sp", "tp")
-    return jax.shard_map(shards, mesh=mesh, in_specs=in_specs, out_specs=out_specs, check_vma=False)
+    return jax.shard_map(chosen, mesh=mesh, in_specs=in_specs, out_specs=out_specs, check_vma=False)

time: 381 us -> 181 us (0.48)
  waiting for transfers between devices: 211 us -> 0.01 us
  Pallas kernels: 0 us -> 163 us
  blocking collectives: 82.7 us -> 0 us
  matrix products: 25.7 us -> 0.15 us
  between operations: 13.5 us -> 0.16 us
  other arithmetic: 15.6 us -> 3.65 us
  local copies, waits for them, and re-layouts: 20.7 us -> 8.8 us
  starting transfers between devices: 10.5 us -> 4.58 us
    all_gather x4 -> x0, waiting for transfers between devices: 182 us -> none  [the longest x1 85.6 us: shards(): arrived = lax.all_gather(received, 'tp', axis=1, tiled=True)]
    pallas_call x0 -> x2, Pallas kernels: none -> 163 us  [the longest x1 140 us: fast_shards(): pl.pallas_call(functools.partial(expert_kernel, nsp, ntp, cap), out_shape...]
    all_to_all x1 -> x0, blocking collectives: 53.3 us -> none  [shards(): lax.all_to_all(send_rows, 'sp', split_axis=0, concat_axis=0, tiled=True)]
    all_to_all x1 -> x0, waiting for transfers between devices: 28.9 us -> none  [shards(): lax.all_to_all(expert_rows, 'sp', split_axis=0, concat_axis=0, tiled=True)]
    dot_general x7 -> x1, matrix products: 25.7 us -> 0.15 us  [dot(): return jnp.dot(a, b, preferred_element_type=F32)]
    psum x2 -> x0, blocking collectives: 15.1 us -> none  [the longest x1 8.19 us: shards(): lax.psum((jnp.sum(conv_sum, axis=1), jnp.sum(conv_sum * conv_sum, axis=1)...]
    all_gather x1 -> x0, blocking collectives: 14.2 us -> none  [shards(): lax.all_gather(shared_hidden, 'tp', axis=1, tiled=True)]
    gather x3 -> x0, local copies, waits for them, and re-layouts: 12.9 us -> none  [the longest x1 7.08 us: shards(): jnp.take(rows_ext, local_slots.reshape(-1), axis=0)]
  transfers between devices with their start and end apart: 6 -> 1, of which waited for: 5 -> 0; matrix products, arithmetic and copies ran while one was open for 3% -> 3% of each run, Pallas kernels for 0% -> 0%
where the time goes in v1:
time: 181 us; the launch traced here: 180 us
  Pallas kernels  163 us (90%)
  local copies, waits for them, and re-layouts  8.8 us (5%)
  starting transfers between devices  4.58 us (3%)
  other arithmetic  3.65 us (2%)
    pallas_call x1, Pallas kernels, fast_shards(): pl.pallas_call(functools.partial(expert_kernel, nsp, ntp, cap), out_shape...  140 us
    pallas_call x1, Pallas kernels, fast_shards(): pl.pallas_call(functools.partial(front_kernel, nsp, ntp), out_shape=[jax....  23.1 us
    ppermute x1, starting transfers between devices, shifted(): return lax.ppermute(block, axis, route)  4.58 us
    unnamed x19, local copies, waits for them, and re-layouts  4.23 us
  transfers between devices with their start and end apart: 1, of which 0 were waited for; matrix products, arithmetic and copies ran while one was open for 3% of the time, Pallas kernels for 0%

profile of v1, /device:TPU:1, one launch (start us, length us, event | category | flops | bytes accessed | tf_op | source)
XLA Modules:
  0.0 180.3 jit_solution(17606289041757809031)
XLA Ops:
  0.0 0.0 copy-start.8
  0.0 1.2 multiply_convert_fusion
  1.2 4.6 %collective-permute-start = (bf16[30,512]{1,0:T(8,128)(2,1)S(1)}, bf16[30,512]{1,0:T(8,128)(2,1)S(1)}, u32[]{:S(2)}, u32[]{:S(2)}) collective-permute-start(bf16[30,512]{1,0:T(8,128)(2,1)S(1)} %slice.268), channel_id=1, source_target_pairs={{0,4},{4,8},{8,12},{12,16},{16,20},{20,24},{24,28},{1,5},{5,9},{9,... | collective-permute-start | bytes 92168 | tf_op jit(solution)/shard_map/ppermute | solution.py:20
  5.8 1.2 fusion.39
  7.0 0.8 fusion.41
  7.7 0.8 fusion.42
  8.5 0.1 fusion.35
  8.7 0.1 copy.18
  8.8 0.1 bitcast_select_fusion
  9.0 0.1 pad.3.clone
  9.1 0.1 maximum_maximum_fusion.route
  9.1 1.0 fusion.40
  10.1 0.7 concatenate.11.poscol
  10.8 0.0 collective-permute-done
  10.8 0.1 pad_maximum_fusion
  10.9 0.1 convert_element_type.31
  10.9 0.0 copy-done.8
  10.9 0.0 copy-start
  11.0 0.0 copy-start.3
  11.0 0.0 copy-start.5
  11.0 0.0 copy-start.6
  11.0 0.0 copy-start.7
  11.0 2.1 %fusion.conv = f32[256,512]{1,0:T(8,128)S(1)} fusion(f32[286,512]{1,0:T(8,128)S(1)} %convert_element_type.31, f32[512]{0:T(512)S(1)} %bitcast.92, f32[512]{0:T(512)S(1)} %bitcast.93, f32[512]{0:T(512)S(1)} %bitcast.64, f32[512]{0:T(512)S(1)} %bitcast.65, f32[512]{0:T(512)S(1)} %bitcast.66, f32[512]{0:T(512)S(1)} %bitcast.67, f32[512]{0:T(512)S(1)} %bitcast.68, ...), kind=kLoop, calls=%fused_computation.1 | loop fusion | flops 8126464 | bytes 16842752 | tf_op jit(solution)/shard_map/add | solution.py:494
  13.1 0.0 copy-done
  13.1 0.1 copy-done.3
  13.3 0.0 copy-done.5
  13.3 0.0 copy-done.6
  13.3 0.0 copy-done.7
  13.3 23.1 %front.1 = (bf16[256,1024]{1,0:T(8,128)(2,1)S(1)}, bf16[256,1024]{1,0:T(8,128)(2,1)S(1)}, f32[8,8,256]{2,1,0:T(8,128)S(1)}) custom-call(f32[256,512]{1,0:T(8,128)S(1)} %fusion.conv, f32[1,512]{1,0:T(1,128)S(1)} %bitcast.49, f32[1,512]{1,0:T(1,128)S(1)} %bitcast.50, bf16[256,1024]{1,0:T(8,128)(2,1)S(1)} %copy-done.3, f32[1,1024]{1,0:T(1,128)S(1)} %bitcast.48, ...), custom_call_target="tpu_custom_call" | custom-call | tf_op jit(solution)/shard_map/front/pallas_call | solution.py:516
  36.4 0.0 copy-start.1
  36.4 0.8 copy-done.1
  37.2 0.0 copy-start.2
  37.2 0.8 copy-done.2
  37.9 0.0 copy-start.4
  38.0 0.6 copy-done.4
  38.6 139.9 %experts.1 = bf16[256,1024]{1,0:T(8,128)(2,1)} custom-call(bf16[256,1024]{1,0:T(8,128)(2,1)} %copy-done.1, bf16[256,1024]{1,0:T(8,128)(2,1)} %copy-done.2, f32[8,8,256]{2,1,0:T(8,128)} %copy-done.4, f32[256,128]{1,0:T(8,128)} %concatenate.11.poscol, bf16[4,1024,256]{2,1,0:T(8,128)(2,1)} %bitcast.51, bf16[4,1024,256]{2,1,0:T(8,128)(2,1)} %bitcast.52, ...), custom_call_target="tpu_custom_call" | custom-call | tf_op jit(solution)/shard_map/experts/pallas_call | solution.py:549
  178.4 1.9 %copy.20 = bf16[256,1024]{1,0:T(8,128)(2,1)} copy(bf16[256,1024]{1,0:T(8,128)(2,1)} %experts.1) | data formatting | bytes 1048576
  (4 shorter events, 0.0 us)
Async XLA Ops:
  0.0 10.9 %copy-start.8 = (f32[512]{0:T(512)S(1)}, f32[512]{0:T(512)}, u32[]{:S(2)}) copy-start(f32[512]{0:T(512)} %param.20) | copy-start | bytes 6148
  1.2 9.6 %collective-permute-start = (bf16[30,512]{1,0:T(8,128)(2,1)S(1)}, bf16[30,512]{1,0:T(8,128)(2,1)S(1)}, u32[]{:S(2)}, u32[]{:S(2)}) collective-permute-start(bf16[30,512]{1,0:T(8,128)(2,1)S(1)} %slice.268), channel_id=1, source_target_pairs={{0,4},{4,8},{8,12},{12,16},{16,20},{20,24},{24,28},{1,5},{5,9},{9,... | collective-permute-start | bytes 92168 | tf_op jit(solution)/shard_map/ppermute | solution.py:20
  10.9 2.2 %copy-start = (bf16[2048,1024]{1,0:T(8,128)(2,1)S(1)}, bf16[2048,1024]{1,0:T(8,128)(2,1)}, u32[]{:S(2)}) copy-start(bf16[2048,1024]{1,0:T(8,128)(2,1)} %param.23) | copy-start | bytes 12582916
  11.0 2.3 %copy-start.3 = (bf16[256,1024]{1,0:T(8,128)(2,1)S(1)}, bf16[256,1024]{1,0:T(8,128)(2,1)}, u32[]{:S(2)}) copy-start(bf16[256,1024]{1,0:T(8,128)(2,1)} %resid.1) | copy-start | bytes 1572868
  11.0 2.3 %copy-start.5 = (f32[1024]{0:T(1024)S(1)}, f32[1024]{0:T(1024)}, u32[]{:S(2)}) copy-start(f32[1024]{0:T(1024)} %param.25) | copy-start | bytes 12292
  11.0 2.3 %copy-start.6 = (f32[512]{0:T(512)S(1)}, f32[512]{0:T(512)}, u32[]{:S(2)}) copy-start(f32[512]{0:T(512)} %param.21) | copy-start | bytes 6148
  11.0 2.3 %copy-start.7 = (f32[512]{0:T(512)S(1)}, f32[512]{0:T(512)}, u32[]{:S(2)}) copy-start(f32[512]{0:T(512)} %param.22) | copy-start | bytes 6148
  36.4 0.8 copy-start.1
  37.2 0.8 copy-start.2
  37.9 0.6 copy-start.4

commit v2 on v1

--- a/solution.py
+++ b/solution.py
@@ -243,7 +243,7 @@
     nsp, ntp, cap,
     normed, mid, route, poscol, wg_h, wu_h, sg_h, su_h, wd_h, sd_h,
     out,
-    buf, wg, wu, sg, su, wd, sd, acc, hid, shid, osend, ret,
+    buf, wg, wu, sg, su, wd, sd, acc, hid, shid, osend, ret, total,
     lsem, recv, zsend, xsend, ysend, relay, dsend, hsend, hrecv, shsend, shrecv, osem, orecv,
 ):
     me = lax.axis_index("sp")
@@ -305,9 +305,6 @@
         copy.start()
     for copy in spread(0, me):
         copy.start()
-    for load in loads:
-        load.wait()
-
     def gate_up(i, b, q, first):
         data = buf[b, q]
         g = dot(data, wg[q])
@@ -323,18 +320,41 @@
         slot = lax.broadcasted_iota(jnp.int32, (cap, tok), 0).astype(F32)
         return jnp.where(slot == route[b, 0:1, :], 1.0, 0.0)
 
-    def hidden_copies(b):
-        return [
-            rcopy(hid.at[b, t], hid.at[b, t], hsend.at[b, j - 1], hrecv.at[b, j - 1],
-                  (me, (t + j) % ntp))
-            for j in range(1, ntp)
+    def gather(ref, part, send, arrive):
+        size = part // 2
+
+        def piece(q, h, sem, device):
+            block = ref.at[q, pl.ds(h * size, size)]
+            return rcopy(block, block, sem, arrive.at[q, h], device)
+
+        first = [
+            piece(t, h, send.at[i, h], (me, peer))
+            for h in range(2)
+            for i, peer in enumerate((t1, t2))
         ]
-
-    def shared_copies():
-        return [
-            rcopy(shid.at[t], shid.at[t], shsend.at[j - 1], shrecv.at[j - 1], (me, (t + j) % ntp))
-            for j in range(1, ntp)
-        ]
+        second = [piece(t1, 0, send.at[2, 0], (me, t2)), piece(t2, 1, send.at[2, 1], (me, t1))]
+
+        def wait(q, h):
+            piece(q, h, send.at[0, 0], (me, t1)).wait_recv()
+
+        def forward():
+            wait(t1, 0)
+            second[0].start()
+            wait(t2, 1)
+            second[1].start()
+
+        def finish():
+            wait(t1, 1)
+            wait(t2, 0)
+            wait(t3, 0)
+            wait(t3, 1)
+
+        return first, second, forward, finish
+
+    def hidden_gather(b):
+        return gather(hid.at[b], cap, hsend.at[b], hrecv.at[b])
+
+    shared_gather = gather(shid, tok, shsend, shrecv)
 
     def gated(g, u):
         return (g / (1.0 + jnp.exp(-g)) * u).astype(BF16)
@@ -342,17 +362,12 @@
     def finish(i, b):
         hs = dot(selection(b).astype(BF16), gated(acc[i, 0], acc[i, 1]))
         hid[b, t] = hs.astype(BF16)
-        for copy in hidden_copies(b):
-            copy.start()
 
     def home(b):
         return rcopy(osend.at[b], ret.at[me], osem.at[b], orecv.at[me], (b, t))
 
     def down(b):
-        for j in range(1, ntp):
-            q = (t - j + ntp) % ntp
-            rcopy(hid.at[b, q], hid.at[b, q], hsend.at[b, j - 1], hrecv.at[b, j - 1],
-                  (me, t1)).wait_recv()
+        hidden_gather(b)[3]()
         o = dot(hid[b, 0], wd[0])
         for q in range(1, ntp):
             o = o + dot(hid[b, q], wd[q])
@@ -378,6 +393,19 @@
                     forward[1].start()
                 across(k, b, 2, t2, h).start()
 
+        @pl.when(k > 1)
+        def _():
+            def one(i, state):
+                hidden_gather(2 * ((z - k + 1 + nz) % nz) + i)[2]()
+                return state
+
+            lax.fori_loop(0, 2, one, 0)
+
+        @pl.when(k < nz)
+        def _():
+            b = 2 * zk + c
+            pb = 2 * zk + 1 - c
+
             @pl.when(k < nz - 1)
             def _():
                 bn = 2 * ((z - k - 1 + nz) % nz) + c
@@ -386,6 +414,11 @@
                 for copy in spread(k + 1, bn):
                     copy.start()
 
+            @pl.when(k == 0)
+            def _():
+                loads[0].wait()
+                loads[1].wait()
+
             gate_up(0, b, t, True)
             gate_up(0, b, t1, False)
             gate_up(0, b, t2, False)
@@ -393,6 +426,27 @@
                 for h in range(2):
                     arrived(pb, q, h)
                 gate_up(1, pb, q, i == 0)
+        @pl.when(k == 2)
+        def _():
+            loads[4].wait()
+            loads[5].wait()
+
+        @pl.when(k > 1)
+        def _():
+            zp = (z - k + 1 + nz) % nz
+
+            def one(i, state):
+                b = 2 * zp + i
+                osend[b] = down(b)
+                home(b).start()
+                return state
+
+            lax.fori_loop(0, 2, one, 0)
+
+        @pl.when(k < nz)
+        def _():
+            b = 2 * zk + c
+            pb = 2 * zk + 1 - c
             for h in range(2):
                 arrived(b, t3, h)
                 across(k, b, 3, t3, h).start()
@@ -403,6 +457,16 @@
             gate_up(1, pb, t3, False)
             finish(1, pb)
 
+            @pl.when(k > 0)
+            def _():
+                for copy in hidden_gather(b)[0] + hidden_gather(pb)[0]:
+                    copy.start()
+
+            @pl.when(k == nz - 1)
+            def _():
+                for copy in hidden_gather(me)[0] + hidden_gather(partner)[0] + shared_gather[0]:
+                    copy.start()
+
         @pl.when(k == 0)
         def _():
             def quarter(q, state):
@@ -413,41 +477,29 @@
                 acc[0, 1] = jnp.where(q == 0, u, acc[0, 1] + u)
                 return state
 
+            loads[2].wait()
+            loads[3].wait()
             lax.fori_loop(0, ntp, quarter, 0)
             shid[t] = gated(acc[0, 0], acc[0, 1])
-            for copy in shared_copies():
-                copy.start()
-
-        @pl.when(k == 1)
-        def _():
-            ret[me] = down(me)
-            osend[partner] = down(partner)
-            home(partner).start()
-
-        @pl.when(k > 1)
-        def _():
-            zp = (z - k + 1 + nz) % nz
-
-            def one(i, state):
-                b = 2 * zp + i
-                osend[b] = down(b)
-                home(b).start()
-                return state
-
-            lax.fori_loop(0, 2, one, 0)
 
         return carry
 
     lax.fori_loop(0, nz + 1, step, 0)
 
-    for copy in shared_copies():
+    hidden_gather(me)[2]()
+    hidden_gather(partner)[2]()
+    shared_gather[2]()
+    osend[partner] = down(partner)
+    home(partner).start()
+    ret[me] = down(me)
+    shared_gather[3]()
+    o = dot(shid[0], sd[0])
+    for q in range(1, ntp):
+        o = o + dot(shid[q], sd[q])
+    total[...] = mid[...].astype(F32) + o
+
+    for copy in shared_gather[0] + shared_gather[1]:
         copy.wait_send()
-    for j in range(1, ntp):
-        q = (t - j + ntp) % ntp
-        rcopy(shid.at[q], shid.at[q], shsend.at[j - 1], shrecv.at[j - 1], (me, t1)).wait_recv()
-    total = mid[...].astype(F32)
-    for q in range(ntp):
-        total = total + dot(shid[q], sd[q])
 
     def drain(k, carry):
         b = 2 * ((z - k + nz) % nz) + c
@@ -463,7 +515,7 @@
         copy.wait_send()
 
     def drain_hidden(b, carry):
-        for copy in hidden_copies(b):
+        for copy in hidden_gather(b)[0] + hidden_gather(b)[1]:
             copy.wait_send()
         return carry
 
@@ -472,10 +524,11 @@
         e = (me + j) % nsp
         rcopy(osend.at[e], ret.at[e], osem.at[e], orecv.at[e], (e, t)).wait()
     lane = lax.broadcasted_iota(jnp.int32, (tok, cap), 1).astype(F32)
+    result = total[...]
     for e in range(nsp):
         pick = jnp.where(lane == poscol[:, e : e + 1], 1.0, 0.0).astype(BF16)
-        total = total + dot(pick, ret[e])
-    out[...] = total.astype(BF16)
+        result = result + dot(pick, ret[e])
+    out[...] = result.astype(BF16)
 
 
 def fast_shards(
@@ -564,13 +617,14 @@
             VMEM((ntp, tok, sw), BF16),
             VMEM((nsp, cap, width), BF16),
             VMEM((nsp, cap, width), BF16),
+            VMEM((tok, width), F32),
             DMA((7,)),
             DMA((nsp, ntp, 2)),
             DMA((nz - 1, 2)),
             DMA((nz, 2)), DMA((nz, 2)), DMA((nz, 2)),
             DMA((nz, ntp, 2)),
-            DMA((nsp, ntp - 1)), DMA((nsp, ntp - 1)),
-            DMA((ntp - 1,)), DMA((ntp - 1,)),
+            DMA((nsp, 3, 2)), DMA((nsp, ntp, 2)),
+            DMA((3, 2)), DMA((ntp, 2)),
             DMA((nsp,)), DMA((nsp,)),
         ],
         compiler_params=pltpu.CompilerParams(

time: 181 us -> 168 us (0.928)
  Pallas kernels: 163 us -> 150 us
    pallas_call x1, Pallas kernels: 140 us -> 127 us  [fast_shards(): pl.pallas_call(functools.partial(expert_kernel, nsp, ntp, cap), out_shape...]
where the time goes in v2:
time: 168 us
  Pallas kernels  150 us (89%)
  local copies, waits for them, and re-layouts  8.8 us (5%)
  starting transfers between devices  4.58 us (3%)
  other arithmetic  3.65 us (2%)
    pallas_call x1, Pallas kernels, fast_shards(): pl.pallas_call(functools.partial(expert_kernel, nsp, ntp, cap), out_shape...  127 us
    pallas_call x1, Pallas kernels, fast_shards(): pl.pallas_call(functools.partial(front_kernel, nsp, ntp), out_shape=[jax....  23.1 us
    ppermute x1, starting transfers between devices, shifted(): return lax.ppermute(block, axis, route)  4.58 us
    unnamed x19, local copies, waits for them, and re-layouts  4.23 us
  transfers between devices with their start and end apart: 1, of which 0 were waited for; matrix products, arithmetic and copies ran while one was open for 3% of the time, Pallas kernels for 0%

profile of v2, /device:TPU:1, one launch (start us, length us, event | category | flops | bytes accessed | tf_op | source)
XLA Modules:
  0.0 167.6 jit_solution(6297342921356826964)
XLA Ops:
  0.0 0.0 copy-start.8
  0.0 1.2 multiply_convert_fusion
  1.2 4.6 %collective-permute-start = (bf16[30,512]{1,0:T(8,128)(2,1)S(1)}, bf16[30,512]{1,0:T(8,128)(2,1)S(1)}, u32[]{:S(2)}, u32[]{:S(2)}) collective-permute-start(bf16[30,512]{1,0:T(8,128)(2,1)S(1)} %slice.268), channel_id=1, source_target_pairs={{0,4},{4,8},{8,12},{12,16},{16,20},{20,24},{24,28},{1,5},{5,9},{9,... | collective-permute-start | bytes 92168 | tf_op jit(solution)/shard_map/ppermute | solution.py:20
  5.8 1.2 fusion.39
  7.0 0.8 fusion.41
  7.7 0.8 fusion.42
  8.5 0.1 fusion.35
  8.7 0.1 copy.18
  8.8 0.1 bitcast_select_fusion
  9.0 0.1 pad.3.clone
  9.1 0.1 maximum_maximum_fusion.route
  9.1 1.0 fusion.40
  10.1 0.7 concatenate.11.poscol
  10.8 0.0 collective-permute-done
  10.8 0.1 pad_maximum_fusion
  10.9 0.1 convert_element_type.31
  10.9 0.0 copy-done.8
  10.9 0.0 copy-start
  11.0 0.0 copy-start.3
  11.0 0.0 copy-start.5
  11.0 0.0 copy-start.6
  11.0 0.0 copy-start.7
  11.0 2.1 %fusion.conv = f32[256,512]{1,0:T(8,128)S(1)} fusion(f32[286,512]{1,0:T(8,128)S(1)} %convert_element_type.31, f32[512]{0:T(512)S(1)} %bitcast.92, f32[512]{0:T(512)S(1)} %bitcast.93, f32[512]{0:T(512)S(1)} %bitcast.64, f32[512]{0:T(512)S(1)} %bitcast.65, f32[512]{0:T(512)S(1)} %bitcast.66, f32[512]{0:T(512)S(1)} %bitcast.67, f32[512]{0:T(512)S(1)} %bitcast.68, ...), kind=kLoop, calls=%fused_computation.1 | loop fusion | flops 8126464 | bytes 16842752 | tf_op jit(solution)/shard_map/add | solution.py:547
  13.1 0.0 copy-done
  13.1 0.1 copy-done.3
  13.3 0.0 copy-done.5
  13.3 0.0 copy-done.6
  13.3 0.0 copy-done.7
  13.3 23.1 %front.1 = (bf16[256,1024]{1,0:T(8,128)(2,1)S(1)}, bf16[256,1024]{1,0:T(8,128)(2,1)S(1)}, f32[8,8,256]{2,1,0:T(8,128)S(1)}) custom-call(f32[256,512]{1,0:T(8,128)S(1)} %fusion.conv, f32[1,512]{1,0:T(1,128)S(1)} %bitcast.49, f32[1,512]{1,0:T(1,128)S(1)} %bitcast.50, bf16[256,1024]{1,0:T(8,128)(2,1)S(1)} %copy-done.3, f32[1,1024]{1,0:T(1,128)S(1)} %bitcast.48, ...), custom_call_target="tpu_custom_call" | custom-call | tf_op jit(solution)/shard_map/front/pallas_call | solution.py:569
  36.4 0.0 copy-start.1
  36.4 0.8 copy-done.1
  37.2 0.0 copy-start.2
  37.2 0.8 copy-done.2
  37.9 0.0 copy-start.4
  38.0 0.6 copy-done.4
  38.6 127.2 %experts.1 = bf16[256,1024]{1,0:T(8,128)(2,1)} custom-call(bf16[256,1024]{1,0:T(8,128)(2,1)} %copy-done.1, bf16[256,1024]{1,0:T(8,128)(2,1)} %copy-done.2, f32[8,8,256]{2,1,0:T(8,128)} %copy-done.4, f32[256,128]{1,0:T(8,128)} %concatenate.11.poscol, bf16[4,1024,256]{2,1,0:T(8,128)(2,1)} %bitcast.51, bf16[4,1024,256]{2,1,0:T(8,128)(2,1)} %bitcast.52, ...), custom_call_target="tpu_custom_call" | custom-call | tf_op jit(solution)/shard_map/experts/pallas_call | solution.py:602
  165.8 1.9 %copy.20 = bf16[256,1024]{1,0:T(8,128)(2,1)} copy(bf16[256,1024]{1,0:T(8,128)(2,1)} %experts.1) | data formatting | bytes 1048576
  (4 shorter events, 0.0 us)
Async XLA Ops:
  0.0 10.9 %copy-start.8 = (f32[512]{0:T(512)S(1)}, f32[512]{0:T(512)}, u32[]{:S(2)}) copy-start(f32[512]{0:T(512)} %param.20) | copy-start | bytes 6148
  1.2 9.6 %collective-permute-start = (bf16[30,512]{1,0:T(8,128)(2,1)S(1)}, bf16[30,512]{1,0:T(8,128)(2,1)S(1)}, u32[]{:S(2)}, u32[]{:S(2)}) collective-permute-start(bf16[30,512]{1,0:T(8,128)(2,1)S(1)} %slice.268), channel_id=1, source_target_pairs={{0,4},{4,8},{8,12},{12,16},{16,20},{20,24},{24,28},{1,5},{5,9},{9,... | collective-permute-start | bytes 92168 | tf_op jit(solution)/shard_map/ppermute | solution.py:20
  10.9 2.2 %copy-start = (bf16[2048,1024]{1,0:T(8,128)(2,1)S(1)}, bf16[2048,1024]{1,0:T(8,128)(2,1)}, u32[]{:S(2)}) copy-start(bf16[2048,1024]{1,0:T(8,128)(2,1)} %param.23) | copy-start | bytes 12582916
  11.0 2.3 %copy-start.3 = (bf16[256,1024]{1,0:T(8,128)(2,1)S(1)}, bf16[256,1024]{1,0:T(8,128)(2,1)}, u32[]{:S(2)}) copy-start(bf16[256,1024]{1,0:T(8,128)(2,1)} %resid.1) | copy-start | bytes 1572868
  11.0 2.3 %copy-start.5 = (f32[1024]{0:T(1024)S(1)}, f32[1024]{0:T(1024)}, u32[]{:S(2)}) copy-start(f32[1024]{0:T(1024)} %param.25) | copy-start | bytes 12292
  11.0 2.3 %copy-start.6 = (f32[512]{0:T(512)S(1)}, f32[512]{0:T(512)}, u32[]{:S(2)}) copy-start(f32[512]{0:T(512)} %param.21) | copy-start | bytes 6148
  11.0 2.3 %copy-start.7 = (f32[512]{0:T(512)S(1)}, f32[512]{0:T(512)}, u32[]{:S(2)}) copy-start(f32[512]{0:T(512)} %param.22) | copy-start | bytes 6148
  36.4 0.8 copy-start.1
  37.2 0.8 copy-start.2
  37.9 0.6 copy-start.4

commit v3 on v2

--- a/solution.py
+++ b/solution.py
@@ -160,22 +160,53 @@
         pl.semaphore_signal(
             barrier, inc=1, device_id=((me + j) % nsp, t), device_id_type=pl.DeviceIdType.MESH
         )
-    pl.semaphore_wait(barrier, ntp - 1 + nsp - 1)
+    return barrier, ntp - 1 + nsp - 1
+
+
+def gather(me, t, ref, part, send, arrive):
+    size = part // 2
+    t1 = t + 1 - 2 * (t % 2)
+    t2 = t + 2 - 4 * (t // 2)
+    t3 = 3 - t
+
+    def piece(q, h, sem, device):
+        block = ref.at[q, pl.ds(h * size, size)]
+        return rcopy(block, block, sem, arrive.at[q, h], device)
+
+    first = [
+        piece(t, h, send.at[i, h], (me, peer))
+        for h in range(2)
+        for i, peer in enumerate((t1, t2))
+    ]
+    second = [piece(t1, 0, send.at[2, 0], (me, t2)), piece(t2, 1, send.at[2, 1], (me, t1))]
+
+    def wait(q, h):
+        piece(q, h, send.at[0, 0], (me, t1)).wait_recv()
+
+    def forward():
+        wait(t1, 0)
+        second[0].start()
+        wait(t2, 1)
+        second[1].start()
+
+    def finish():
+        wait(t1, 1)
+        wait(t2, 0)
+        wait(t3, 0)
+        wait(t3, 1)
+
+    return first, second, forward, finish
 
 
 def front_kernel(
     nsp, ntp,
-    conv, gain, bias, resid, ngain, route, proj_hbm,
-    normed, mid, route_all,
-    proj, gbuf, st, st2, rbuf,
-    lsem, gsend, grecv, ssend, srecv, s2send, s2recv, rsend, rrecv,
+    conv, gain, bias, resid, ngain, route,
+    normed, mid, weights, proj, gbuf, st, st2, rbuf,
+    gsend, grecv, ssend, srecv, s2send, s2recv, rsend, rrecv,
 ):
     me = lax.axis_index("sp")
     t = lax.axis_index("tp")
     tok = conv.shape[0]
-    weights = pltpu.make_async_copy(proj_hbm, proj, lsem.at[0])
-    weights.start()
-    greet(nsp, ntp, me, t)
     tables = []
     for j in range(1, nsp):
         e = (me + j) % nsp
@@ -216,35 +247,32 @@
     var = sums[:, 1:2] / channels - mean * mean
     v = (x - mean) * lax.rsqrt(var + norm_eps) * gain[...] + bias[...]
     gbuf[t] = (v / (1.0 + jnp.exp(-v))).astype(BF16)
-    copies = []
-    for j in range(1, ntp):
-        copy = rcopy(gbuf.at[t], gbuf.at[t], gsend.at[j - 1], grecv.at[j - 1], (me, (t + j) % ntp))
+    first, second, forward, settle = gather(me, t, gbuf, tok, gsend, grecv)
+    for copy in first:
         copy.start()
-        copies.append(copy)
     weights.wait()
     total = resid[...].astype(F32) + dot(gbuf[t], proj[t])
-    for j in range(1, ntp):
-        copies[j - 1].wait_recv()
-        q = (t - j + ntp) % ntp
+    forward()
+    settle()
+    for i in (1, 2, 3):
+        q = (t + i) % ntp
         total = total + dot(gbuf[q], proj[q])
     mid[...] = total.astype(BF16)
     wide = mid[...].astype(F32)
     squares = exchange(st2, [jnp.sum(wide * wide, axis=1, keepdims=True)], s2send, s2recv)
     scale = lax.rsqrt(squares[:, 0:1] / (mid.shape[1] * ntp) + norm_eps)
     normed[...] = (wide * scale * ngain[...]).astype(BF16)
-    for copy in copies:
+    for copy in first + second:
         copy.wait_send()
     for copy in tables:
         copy.wait()
-    route_all[...] = rbuf[...]
 
 
 def expert_kernel(
     nsp, ntp, cap,
-    normed, mid, route, poscol, wg_h, wu_h, sg_h, su_h, wd_h, sd_h,
-    out,
+    normed, mid, route, poscol, loads, out,
     buf, wg, wu, sg, su, wd, sd, acc, hid, shid, osend, ret, total,
-    lsem, recv, zsend, xsend, ysend, relay, dsend, hsend, hrecv, shsend, shrecv, osem, orecv,
+    osem_own, recv, zsend, xsend, ysend, relay, dsend, hsend, hrecv, shsend, shrecv, osem, orecv,
 ):
     me = lax.axis_index("sp")
     t = lax.axis_index("tp")
@@ -258,17 +286,8 @@
     t1 = t + 1 - 2 * (t % 2)
     t2 = t + 2 - 4 * (t // 2)
     t3 = 3 - t
-    loads = [
-        pltpu.make_async_copy(a, b, lsem.at[i])
-        for i, (a, b) in enumerate(
-            [(wg_h, wg), (wu_h, wu), (sg_h, sg), (su_h, su), (wd_h, wd), (sd_h, sd)]
-        )
-    ]
-    own = pltpu.make_async_copy(normed, buf.at[me, t], lsem.at[6])
+    own = pltpu.make_async_copy(normed, buf.at[me, t], osem_own.at[0])
     own.start()
-    for load in loads:
-        load.start()
-    greet(nsp, ntp, me, t)
     own.wait()
 
     def rows(b, q, h):
@@ -320,41 +339,10 @@
         slot = lax.broadcasted_iota(jnp.int32, (cap, tok), 0).astype(F32)
         return jnp.where(slot == route[b, 0:1, :], 1.0, 0.0)
 
-    def gather(ref, part, send, arrive):
-        size = part // 2
-
-        def piece(q, h, sem, device):
-            block = ref.at[q, pl.ds(h * size, size)]
-            return rcopy(block, block, sem, arrive.at[q, h], device)
-
-        first = [
-            piece(t, h, send.at[i, h], (me, peer))
-            for h in range(2)
-            for i, peer in enumerate((t1, t2))
-        ]
-        second = [piece(t1, 0, send.at[2, 0], (me, t2)), piece(t2, 1, send.at[2, 1], (me, t1))]
-
-        def wait(q, h):
-            piece(q, h, send.at[0, 0], (me, t1)).wait_recv()
-
-        def forward():
-            wait(t1, 0)
-            second[0].start()
-            wait(t2, 1)
-            second[1].start()
-
-        def finish():
-            wait(t1, 1)
-            wait(t2, 0)
-            wait(t3, 0)
-            wait(t3, 1)
-
-        return first, second, forward, finish
-
     def hidden_gather(b):
-        return gather(hid.at[b], cap, hsend.at[b], hrecv.at[b])
-
-    shared_gather = gather(shid, tok, shsend, shrecv)
+        return gather(me, t, hid.at[b], cap, hsend.at[b], hrecv.at[b])
+
+    shared_gather = gather(me, t, shid, tok, shsend, shrecv)
 
     def gated(g, u):
         return (g / (1.0 + jnp.exp(-g)) * u).astype(BF16)
@@ -401,6 +389,11 @@
 
             lax.fori_loop(0, 2, one, 0)
 
+        @pl.when(k == nz)
+        def _():
+            for copy in hidden_gather(me)[0] + hidden_gather(partner)[0] + shared_gather[0]:
+                copy.start()
+
         @pl.when(k < nz)
         def _():
             b = 2 * zk + c
@@ -452,6 +445,12 @@
                 across(k, b, 3, t3, h).start()
             gate_up(0, b, t3, False)
             finish(0, b)
+
+            @pl.when(k > 0)
+            def _():
+                for copy in hidden_gather(b)[0]:
+                    copy.start()
+
             for h in range(2):
                 arrived(pb, t3, h)
             gate_up(1, pb, t3, False)
@@ -459,12 +458,7 @@
 
             @pl.when(k > 0)
             def _():
-                for copy in hidden_gather(b)[0] + hidden_gather(pb)[0]:
-                    copy.start()
-
-            @pl.when(k == nz - 1)
-            def _():
-                for copy in hidden_gather(me)[0] + hidden_gather(partner)[0] + shared_gather[0]:
+                for copy in hidden_gather(pb)[0]:
                     copy.start()
 
         @pl.when(k == 0)
@@ -531,6 +525,41 @@
     out[...] = result.astype(BF16)
 
 
+def convolve(padded, taps, bias, conv):
+    tok, ch = conv.shape
+    block = 64
+    for r in range(0, tok, block):
+        for l in range(0, ch, 128):
+            total = jnp.zeros((block, 128), F32) + bias[:, l : l + 128]
+            for i in range(taps.shape[0]):
+                rows = padded[r + i : r + i + block, l : l + 128]
+                total = total + taps[i : i + 1, l : l + 128] * rows
+            conv[r : r + block, l : l + 128] = total
+
+
+def layer_kernel(
+    nsp, ntp, cap,
+    padded, taps, tap_bias, gain, bias, resid, ngain, table, poscol,
+    proj_h, wg_h, wu_h, sg_h, su_h, wd_h, sd_h,
+    out,
+    lsem, conv, normed, mid, rbuf, proj, gbuf, st, st2, *rest,
+):
+    front_sems = rest[:8]
+    rest = rest[8:]
+    pairs = zip((proj_h, wg_h, wu_h, sg_h, su_h, wd_h, sd_h), (proj,) + tuple(rest[1:7]))
+    loads = [pltpu.make_async_copy(a, b, lsem.at[i]) for i, (a, b) in enumerate(pairs)]
+    for load in loads:
+        load.start()
+    barrier, count = greet(nsp, ntp, lax.axis_index("sp"), lax.axis_index("tp"))
+    convolve(padded, taps, tap_bias, conv)
+    pl.semaphore_wait(barrier, count)
+    front_kernel(
+        nsp, ntp, conv, gain, bias, resid, ngain, table,
+        normed, mid, loads[0], proj, gbuf, st, st2, rbuf, *front_sems,
+    )
+    expert_kernel(nsp, ntp, cap, normed, mid, rbuf, poscol, loads[1:], out, *rest)
+
+
 def fast_shards(
     u_val, u_gate, conv_weight, conv_bias, ln_gain, ln_bias, proj_weight, resid, norm_gain,
     route_ids, route_wts, expert_gate, expert_up, expert_down, shared_gate, shared_up, shared_down,
@@ -541,10 +570,11 @@
     taps = conv_weight.shape[0]
     gated = (u_val.astype(F32) * jax.nn.sigmoid(u_gate.astype(F32))).astype(BF16)
     rim = shifted(gated[tok - (taps - 1) :], "sp", 1)
-    padded = lax.optimization_barrier(jnp.concatenate([rim, gated], axis=0)).astype(F32)
-    conv_sum = jnp.zeros((tok, gated.shape[1]), F32) + conv_bias[None, :]
-    for i in range(taps):
-        conv_sum = conv_sum + conv_weight[i][None, :] * padded[i : i + tok]
+    spare = -(tok + taps - 1) % 8
+    padded = jnp.concatenate(
+        [rim, gated, jnp.zeros((spare, gated.shape[1]), BF16)], axis=0
+    ).astype(F32)
+    ch = gated.shape[1]
 
     top = route_ids.shape[1]
     cap = 2 * tok * top // nsp
@@ -562,49 +592,31 @@
     )
     poscol = jnp.concatenate([pos.T, jnp.full((tok, 128 - nsp), -1.0, F32)], axis=1)
 
-    ch = conv_sum.shape[1]
     width = resid.shape[1]
     vm = pl.BlockSpec(memory_space=VMEM)
     hbm = pl.BlockSpec(memory_space=pl.ANY)
-    normed, mid, route_all = pl.pallas_call(
-        functools.partial(front_kernel, nsp, ntp),
-        out_shape=[
-            jax.ShapeDtypeStruct((tok, width), BF16),
-            jax.ShapeDtypeStruct((tok, width), BF16),
-            jax.ShapeDtypeStruct((nsp, 8, tok), F32),
-        ],
-        in_specs=[vm] * 6 + [hbm],
-        out_specs=[vm] * 3,
+    hw = expert_gate.shape[2]
+    sw = shared_gate.shape[1]
+    nz = nsp // 2
+    return pl.pallas_call(
+        functools.partial(layer_kernel, nsp, ntp, cap),
+        out_shape=jax.ShapeDtypeStruct((tok, width), BF16),
+        in_specs=[vm] * 9 + [hbm] * 7,
+        out_specs=vm,
         scratch_shapes=[
+            DMA((7,)),
+            VMEM((tok, ch), F32),
+            VMEM((tok, width), BF16),
+            VMEM((tok, width), BF16),
+            VMEM((nsp, 8, tok), F32),
             VMEM((ntp, ch, width), BF16),
             VMEM((ntp, tok, ch), BF16),
             VMEM((ntp, 8, tok), F32),
             VMEM((ntp, 8, tok), F32),
-            VMEM((nsp, 8, tok), F32),
-            DMA((1,)),
-            DMA((ntp - 1,)), DMA((ntp - 1,)),
+            DMA((3, 2)), DMA((ntp, 2)),
             DMA((ntp - 1,)), DMA((ntp - 1,)),
             DMA((ntp - 1,)), DMA((ntp - 1,)),
             DMA((nsp - 1,)), DMA((nsp - 1,)),
-        ],
-        compiler_params=pltpu.CompilerParams(
-            collective_id=1, has_side_effects=True, vmem_limit_bytes=24 << 20
-        ),
-        name="front",
-    )(
-        conv_sum, ln_gain[None, :], ln_bias[None, :], resid, norm_gain[None, :], table,
-        proj_weight.reshape(ntp, ch, width),
-    )
-
-    hw = expert_gate.shape[2]
-    sw = shared_gate.shape[1]
-    nz = nsp // 2
-    return pl.pallas_call(
-        functools.partial(expert_kernel, nsp, ntp, cap),
-        out_shape=jax.ShapeDtypeStruct((tok, width), BF16),
-        in_specs=[vm] * 4 + [hbm] * 6,
-        out_specs=vm,
-        scratch_shapes=[
             VMEM((nsp, ntp, tok, width), BF16),
             VMEM((ntp, width, hw), BF16),
             VMEM((ntp, width, hw), BF16),
@@ -618,7 +630,7 @@
             VMEM((nsp, cap, width), BF16),
             VMEM((nsp, cap, width), BF16),
             VMEM((tok, width), F32),
-            DMA((7,)),
+            DMA((1,)),
             DMA((nsp, ntp, 2)),
             DMA((nz - 1, 2)),
             DMA((nz, 2)), DMA((nz, 2)), DMA((nz, 2)),
@@ -628,11 +640,12 @@
             DMA((nsp,)), DMA((nsp,)),
         ],
         compiler_params=pltpu.CompilerParams(
-            collective_id=2, has_side_effects=True, vmem_limit_bytes=56 << 20
+            collective_id=1, has_side_effects=True, vmem_limit_bytes=60 << 20
         ),
-        name="experts",
+        name="layer",
     )(
-        normed, mid, route_all, poscol,
+        padded, conv_weight, conv_bias[None, :], ln_gain[None, :], ln_bias[None, :], resid, norm_gain[None, :], table, poscol,
+        proj_weight.reshape(ntp, ch, width),
         expert_gate[0].reshape(ntp, width, hw),
         expert_up[0].reshape(ntp, width, hw),
         shared_gate.reshape(ntp, width, sw),

time: 168 us -> 161 us (0.958)
  local copies, waits for them, and re-layouts: 8.8 us -> 4.36 us
    unnamed x19 -> x1, local copies, waits for them, and re-layouts: 4.23 us -> 1.87 us
    slice x2 -> x0, local copies, waits for them, and re-layouts: 2.17 us -> none  [fast_shards(): conv_sum = conv_sum + conv_weight[i][None, :] * padded[i:i + tok]]
    add x1 -> x0, other arithmetic: 2.1 us -> none  [fast_shards(): conv_sum = conv_sum + conv_weight[i][None, :] * padded[i:i + tok]]
    pallas_call x2 -> x1, Pallas kernels: 150 us -> 149 us  [fast_shards(): pl.pallas_call(functools.partial(layer_kernel, nsp, ntp, cap), out_shape=...]
  transfers between devices with their start and end apart: 1 -> 1, of which waited for: 0 -> 0; matrix products, arithmetic and copies ran while one was open for 3% -> 2% of each run, Pallas kernels for 0% -> 0%
where the time goes in v3:
time: 161 us
  Pallas kernels  149 us (93%)
  starting transfers between devices  4.58 us (3%)
  local copies, waits for them, and re-layouts  4.36 us (3%)
  other arithmetic  2.96 us (2%)
    pallas_call x1, Pallas kernels, fast_shards(): pl.pallas_call(functools.partial(layer_kernel, nsp, ntp, cap), out_shape=...  149 us
    ppermute x1, starting transfers between devices, shifted(): return lax.ppermute(block, axis, route)  4.58 us
  transfers between devices with their start and end apart: 1, of which 0 were waited for; matrix products, arithmetic and copies ran while one was open for 2% of the time, Pallas kernels for 0%

profile of v3, /device:TPU:1, one launch (start us, length us, event | category | flops | bytes accessed | tf_op | source)
XLA Modules:
  0.0 161.0 jit_solution(12674661441059026989)
XLA Ops:
  0.0 1.2 multiply_convert_fusion
  1.2 4.6 %collective-permute-start = (bf16[30,512]{1,0:T(8,128)(2,1)S(1)}, bf16[30,512]{1,0:T(8,128)(2,1)S(1)}, u32[]{:S(2)}, u32[]{:S(2)}) collective-permute-start(bf16[30,512]{1,0:T(8,128)(2,1)S(1)} %slice.20), channel_id=1, source_target_pairs={{0,4},{4,8},{8,12},{12,16},{16,20},{20,24},{24,28},{1,5},{5,9},{9,... | collective-permute-start | bytes 92168 | tf_op jit(solution)/shard_map/ppermute | solution.py:20
  5.8 0.8 fusion.8
  6.6 0.8 fusion.9
  7.3 0.1 fusion.4
  7.5 0.1 copy.18
  7.6 0.1 bitcast_select_fusion
  7.8 0.1 pad.3.clone
  7.9 0.7 maximum_maximum_fusion.table
  8.6 0.1 pad.6.clone
  8.6 0.7 concatenate.11.poscol
  9.3 0.0 collective-permute-done
  9.3 0.9 maximum_convert_fusion.padded
  10.2 148.9 %layer.1 = bf16[256,1024]{1,0:T(8,128)(2,1)} custom-call(f32[288,512]{1,0:T(8,128)} %maximum_convert_fusion.padded, f32[31,512]{1,0:T(8,128)} %taps.1, f32[1,512]{1,0:T(1,128)} %bitcast.33, f32[1,512]{1,0:T(1,128)} %bitcast.34, f32[1,512]{1,0:T(1,128)} %bitcast.35, bf16[256,1024]{1,0:T(8,128)(2,1)} %resid.1, f32[1,1024]{1,0:T(1,128)} %bitcast.30, ...), custom_call_target="tpu_custom_call" | custom-call | tf_op jit(solution)/shard_map/layer/pallas_call | solution.py:601
  159.1 1.9 %copy.20 = bf16[256,1024]{1,0:T(8,128)(2,1)} copy(bf16[256,1024]{1,0:T(8,128)(2,1)} %layer.1) | data formatting | bytes 1048576
  (5 shorter events, 0.0 us)
Async XLA Ops:
  1.2 8.1 %collective-permute-start = (bf16[30,512]{1,0:T(8,128)(2,1)S(1)}, bf16[30,512]{1,0:T(8,128)(2,1)S(1)}, u32[]{:S(2)}, u32[]{:S(2)}) collective-permute-start(bf16[30,512]{1,0:T(8,128)(2,1)S(1)} %slice.20), channel_id=1, source_target_pairs={{0,4},{4,8},{8,12},{12,16},{16,20},{20,24},{24,28},{1,5},{5,9},{9,... | collective-permute-start | bytes 92168 | tf_op jit(solution)/shard_map/ppermute | solution.py:20
